TPU v7x, 32 devices: a whole 2x2x4 slice. The times are simulated.
32 devices in a mesh: sp: 8 (over z, core), tp: 4 (over y, x).
Axes of the slice: x: 2, y: 2, z: 4, core: 2. Of those that a mesh axis runs over, the one named last changes fastest.
Arguments:
- cell_query_heads: bfloat16 [1024, 2048], P('sp', 'tp'), may hold values from -6 to 6
- cell_key_heads: bfloat16 [1024, 2048], P('sp', 'tp'), may hold values from -6 to 6
- cell_value_heads: bfloat16 [1024, 2048], P('sp', 'tp'), may hold values from -6 to 6
- output_gate_logits: bfloat16 [1024, 2048], P('sp', 'tp'), may hold values from -6 to 6
- input_gate_log: float32 [1024, 16], P('sp', 'tp'), may hold values from -7 to 310
- forget_gate_logits: float32 [1024, 16], P('sp', 'tp'), may hold values from 1 to 14
- extra_log_decay: float32 [1024, 16], P('sp', 'tp'), may hold values from -1 to 0
- documents: int32 [1024], P('sp'), may hold values from 0 to 7, never falling along the last dimension, each value on 1 to 256 neighbouring positions
- head_norm_gain: float32 [2048], P('tp'), may hold values from 0.1 to 1.9
- stream: bfloat16 [1024, 4096], P('sp', 'tp'), may hold values from -6 to 6
- output_weight: bfloat16 [2048, 4096], P(None, 'tp'), may hold values from -0.125 to 0.125
- expert_norm_gain: bfloat16 [4096], P('tp'), may hold values from 0.099609375 to 1.8984375
- expert_choice_index: int32 [1024, 2], P('sp'), may hold values from 0 to 7, all different within a row; in each aligned block of 128 rows (0 to 127, 128 to 255, ...) at most 64 rows name the same one
- routing_weight: float32 [1024, 2], P('sp'), may hold values from 0.2 to 1
- gate_weight: bfloat16 [8, 4096, 2048], P('sp', None, 'tp'), may hold values from -0.09375 to 0.09375
- up_weight: bfloat16 [8, 4096, 2048], P('sp', None, 'tp'), may hold values from -0.09375 to 0.09375
- down_weight: bfloat16 [8, 2048, 4096], P('sp', None, 'tp'), may hold values from -0.125 to 0.125
Outputs:
- output: bfloat16 [1024, 4096], P('sp', 'tp')
Inputs may be any that keep to these rules, and one draw needn't show every extreme that they name: `expert_choice_index`: in the rows of one index of sp no expert is named more than 64 times, a bound that some block reaches. `documents`: never falling; each document 1 to 256 positions, one exactly 256.
All inputs are finite; a program needn't handle non-finite values.
Results may differ from a plain program's by a relative error of at most 0.01.
Values may be sent and summed in bfloat16 or wider, within the bound.
A program may use at most 64 MiB of HBM per device.

v0:
```python
import jax
import jax.numpy as jnp
from jax import lax
from jax.sharding import PartitionSpec as P

D = 4096
HD = 128
TOPK = 2


EPSILON = 1e-06
LOW_LOG = -1e30
HIGHEST = lax.Precision.HIGHEST


def prefix_2(part, axis, combine, identity):
    place = lax.axis_index(axis)
    gathered = jax.tree.map(lambda a: lax.all_gather(a, axis), part)
    state = jax.tree.map(lambda a, e: jnp.zeros_like(a) + jnp.asarray(e, a.dtype), part, identity)

    def one(turn, state):
        return combine(
            state, jax.tree.map(lambda a: lax.dynamic_index_in_dim(a, turn, 0, False), gathered)
        )

    return lax.fori_loop(0, place, one, state)


def empty_summary(heads, width):
    return (
        jnp.zeros((heads, width, width), jnp.float32),
        jnp.zeros((heads, width), jnp.float32),
        jnp.full((heads,), LOW_LOG, jnp.float32),
        jnp.zeros((heads,), jnp.float32),
        jnp.zeros((), jnp.int32),
        jnp.full((), -1, jnp.int32),
        jnp.full((), -1, jnp.int32),
    )


def block_summary(key_f, value_f, decay_logarithm, input_gate_log, documents, first_global):
    length = documents.shape[0]
    positions = jnp.arange(length, dtype=jnp.int32)
    cumulative = jnp.cumsum(decay_logarithm, axis=0)
    total_log = cumulative[-1]
    prior_log = cumulative - decay_logarithm
    starts = jnp.concatenate([jnp.reshape(first_global, (1,)), documents[1:] != documents[:-1]])
    inside = jnp.any(starts)
    last_start = jnp.max(jnp.where(starts, positions, -1))
    base_log = jnp.sum(jnp.where((positions == last_start)[:, None], prior_log, 0.0), axis=0)
    in_last = (documents == documents[-1])[:, None]
    weight_log = total_log[None, :] - cumulative + input_gate_log
    peak_log = jnp.max(jnp.where(in_last, weight_log, LOW_LOG), axis=0)
    peak_log = jnp.where(inside, jnp.maximum(peak_log, total_log - base_log), peak_log)
    weights = jnp.where(in_last, jnp.exp(jnp.minimum(weight_log - peak_log[None, :], 0.0)), 0.0)
    matrix = jnp.einsum("lhd,lhe->hde", weights[:, :, None] * key_f, value_f, precision=HIGHEST)
    normer = jnp.sum(weights[:, :, None] * key_f, axis=0)
    return (
        matrix,
        normer,
        peak_log,
        total_log,
        inside.astype(jnp.int32),
        documents[0],
        documents[-1],
    )


def combine(early, late):
    broken = late[5] != early[6]
    carry_matrix = jnp.where(broken, 0.0, early[0])
    carry_normer = jnp.where(broken, 0.0, early[1])
    carry_peak = jnp.where(broken, 0.0, early[2])
    joined = jnp.maximum(late[3] + carry_peak, late[2])
    older = jnp.exp(late[3] + carry_peak - joined)
    newer = jnp.exp(late[2] - joined)
    resets = late[4] > 0
    matrix = jnp.where(
        resets, late[0], older[:, None, None] * carry_matrix + newer[:, None, None] * late[0]
    )
    normer = jnp.where(resets, late[1], older[:, None] * carry_normer + newer[:, None] * late[1])
    peak_log = jnp.where(resets, late[2], joined)
    flags = jnp.maximum(jnp.maximum(early[4], late[4]), broken.astype(jnp.int32))
    merged = (matrix, normer, peak_log, early[3] + late[3], flags, early[5], late[6])
    early_empty = early[6] < 0
    late_empty = late[6] < 0
    return tuple(
        (
            jnp.where(early_empty, second, jnp.where(late_empty, first_item, joint))
            for first_item, second, joint in zip(early, late, merged)
        )
    )


def block_output(query_f, key_f, value_f, decay_logarithm, input_gate_log, documents, prefix):
    prev_matrix, prev_normer, prev_peak, _, _, _, prev_last = prefix
    length = documents.shape[0]
    positions = jnp.arange(length, dtype=jnp.int32)
    cumulative = jnp.cumsum(decay_logarithm, axis=0)
    prior_log = cumulative - decay_logarithm
    before = jnp.concatenate([jnp.reshape(prev_last, (1,)), documents[:-1]])
    starts = documents != before
    last_start = lax.cummax(jnp.where(starts, positions, -1), axis=0)
    started = last_start >= 0
    picker = (positions[None, :] == last_start[:, None]).astype(jnp.float32)
    base_log = jnp.dot(picker, prior_log, precision=HIGHEST)
    carry_log = (cumulative + jnp.where(started[:, None], -base_log, prev_peak[None, :])).T
    same_doc = (documents[:, None] == documents[None, :]) & (
        positions[:, None] >= positions[None, :]
    )
    cum_heads = cumulative.T
    pair_log = cum_heads[:, :, None] - cum_heads[:, None, :] + input_gate_log.T[:, None, :]
    pair_log = jnp.where(same_doc[None], pair_log, LOW_LOG)
    peak_log = jnp.maximum(carry_log, jnp.max(pair_log, axis=-1))
    weights = jnp.exp(pair_log - peak_log[:, :, None])
    scores = jnp.einsum("lhd,shd->hls", query_f, key_f, precision=HIGHEST) * weights
    carry_scale = jnp.where(started[None, :], 0.0, jnp.exp(carry_log - peak_log))
    numer = jnp.einsum("hls,she->hle", scores, value_f, precision=HIGHEST)
    numer = numer + carry_scale[:, :, None] * jnp.einsum(
        "lhd,hde->hle", query_f, prev_matrix, precision=HIGHEST
    )
    denom = jnp.sum(scores, axis=-1) + carry_scale * jnp.einsum(
        "lhd,hd->hl", query_f, prev_normer, precision=HIGHEST
    )
    cell_vals = numer / jnp.maximum(jnp.abs(denom), jnp.exp(-peak_log))[:, :, None]
    return jnp.transpose(cell_vals, (1, 0, 2))


def finish_cell(cell_vals, output_gate_logits, head_norm_gain):
    length, heads, width = cell_vals.shape
    gated_cell = (
        jax.nn.sigmoid(output_gate_logits.astype(jnp.float32)).reshape(length, heads, width)
        * cell_vals
    )
    scaled = gated_cell * lax.rsqrt(
        jnp.mean(gated_cell * gated_cell, axis=-1, keepdims=True) + EPSILON
    )
    scaled = scaled * head_norm_gain.reshape(heads, width)
    return scaled.reshape(length, heads * width).astype(jnp.bfloat16)


def expert_work(row_block, gate_weight, up_weight, down_weight):
    gate_act = jnp.einsum(
        "sqid,qdf->sqif", row_block, gate_weight, preferred_element_type=jnp.float32
    )
    upward = jnp.einsum("sqid,qdf->sqif", row_block, up_weight, preferred_element_type=jnp.float32)
    hidden = (jax.nn.silu(gate_act) * upward).astype(jnp.bfloat16)
    result = jnp.einsum(
        "sqif,qfe->sqie",
        lax.all_gather(hidden, "tp", axis=3, tiled=True),
        down_weight,
        preferred_element_type=jnp.float32,
    )
    return result.astype(jnp.bfloat16)


def per_device(
    cell_query_heads,
    cell_key_heads,
    cell_value_heads,
    output_gate_logits,
    input_gate_log,
    forget_gate_logits,
    extra_log_decay,
    documents,
    head_norm_gain,
    stream,
    output_weight,
    expert_norm_gain,
    expert_choice_index,
    routing_weight,
    gate_weight,
    up_weight,
    down_weight,
):
    tokens = documents.shape[0]
    local_heads = input_gate_log.shape[1]
    shaped = (tokens, local_heads, HD)
    query_f = cell_query_heads.astype(jnp.float32).reshape(shaped)
    key_f = cell_key_heads.astype(jnp.float32).reshape(shaped) * HD ** (-0.5)
    value_f = cell_value_heads.astype(jnp.float32).reshape(shaped)
    decay_logarithm = jax.nn.log_sigmoid(forget_gate_logits) + extra_log_decay
    first_global = lax.axis_index("sp") == 0
    summary = block_summary(
        key_f, value_f, decay_logarithm, input_gate_log, documents, first_global
    )
    prefix = prefix_2(summary, "sp", combine, empty_summary(local_heads, HD))
    cell_vals = block_output(
        query_f, key_f, value_f, decay_logarithm, input_gate_log, documents, prefix
    )
    memory_cell_output = finish_cell(cell_vals, output_gate_logits, head_norm_gain)
    projected = jnp.dot(
        lax.all_gather(memory_cell_output, "tp", axis=1, tiled=True),
        output_weight,
        preferred_element_type=jnp.float32,
    )
    resid = (stream.astype(jnp.float32) + projected).astype(jnp.bfloat16)
    groups = lax.axis_size("sp")
    experts_all = groups * gate_weight.shape[0]
    capacity = 2 * tokens * TOPK // experts_all
    flat_ids = expert_choice_index.reshape(-1)
    onehot = (flat_ids[:, None] == jnp.arange(experts_all, dtype=jnp.int32)[None, :]).astype(
        jnp.int32
    )
    rank_in = jnp.sum((jnp.cumsum(onehot, axis=0) - onehot) * onehot, axis=1)
    slot_of = (flat_ids * capacity + rank_in).reshape(tokens, TOPK)
    slot_index = jnp.arange(experts_all * capacity, dtype=jnp.int32)
    chooser = jnp.any(slot_index[:, None, None] == slot_of[None, :, :], axis=2).astype(jnp.bfloat16)
    bucket_shape = (groups, gate_weight.shape[0], capacity)
    rows_f = resid.astype(jnp.float32)
    squares = lax.psum(jnp.sum(rows_f * rows_f, axis=1), "tp")
    normed = rows_f * lax.rsqrt(squares[:, None] / D + EPSILON)
    normed = (normed * expert_norm_gain.astype(jnp.float32)[None, :]).astype(jnp.bfloat16)
    packed = jnp.dot(chooser, normed, preferred_element_type=jnp.float32).astype(jnp.bfloat16)
    packed = packed.reshape(bucket_shape + (normed.shape[1],))
    row_block = lax.all_gather(
        lax.all_to_all(packed, "sp", split_axis=0, concat_axis=0, tiled=True),
        "tp",
        axis=3,
        tiled=True,
    )
    served = expert_work(row_block, gate_weight, up_weight, down_weight)
    returned = lax.all_to_all(served, "sp", split_axis=0, concat_axis=0, tiled=True).reshape(
        -1, served.shape[3]
    )
    mixed = resid.astype(jnp.float32)
    for ordinal in range(TOPK):
        selector = (slot_of[:, ordinal][:, None] == slot_index[None, :]).astype(jnp.bfloat16)
        picked = jnp.dot(selector, returned, preferred_element_type=jnp.float32)
        mixed = mixed + routing_weight[:, ordinal : ordinal + 1] * picked
    return mixed.astype(jnp.bfloat16)


def solution(mesh):
    placed = (
        P("sp", "tp"),
        P("sp", "tp"),
        P("sp", "tp"),
        P("sp", "tp"),
        P("sp", "tp"),
        P("sp", "tp"),
        P("sp", "tp"),
        P("sp"),
        P("tp"),
        P("sp", "tp"),
        P(None, "tp"),
        P("tp"),
        P("sp", None),
        P("sp", None),
        P("sp", None, "tp"),
        P("sp", None, "tp"),
        P("sp", None, "tp"),
    )
    return jax.shard_map(
        per_device, mesh=mesh, in_specs=placed, out_specs=P("sp", "tp"), check_vma=False
    )
```

profile of v0, /device:TPU:0, one launch (start us, length us, event | category | flops | bytes accessed | tf_op | source)
XLA Modules:
  0.0 303.4 jit_solution(6847889655338509931)
XLA Ops:
  6.6 0.8 fusion.74
  7.5 0.2 reduce_window_sum.27
  7.7 1.5 fusion.81
  9.2 1.3 dynamic-slice
  10.5 2.0 slice_dynamic-update-slice_fusion
  12.5 1.3 broadcast_compare_fusion.1
  13.8 0.7 fusion.78
  14.5 0.6 iota_compare_fusion.10
  15.7 0.9 select_reduce_fusion
  16.7 0.8 select_multiply_fusion
  17.4 1.0 copy.177
  18.5 1.0 copy.183
  19.5 1.1 fusion.61
  20.7 0.7 dynamic-update-slice.1
  21.4 1.4 slice_dynamic-update-slice_fusion.1
  22.8 10.6 %all-reduce.3 = (s32[8]{0:T(128)S(1)}, s32[8]{0:T(128)S(1)}, s32[8]{0:T(128)S(1)}) all-reduce(s32[8]{0:T(128)S(1)} %slice_dynamic-update-slice_fusion.1, s32[8]{0:T(128)S(1)} %dynamic-update-slice.1, s32[8]{0:T(128)S(1)} %get-tuple-element.244), channel_id=1, replica_groups=mesh['sp'=8,'tp'=4] {'sp'}, use_global_device_ids=true, to_apply=%add | all-reduce | flops 24 | bytes 192
  33.4 0.8 copy.162
  34.2 0.1 eq.129
  34.4 0.1 eq.125
  34.7 1.0 copy.176
  35.7 1.0 add_divide_fusion
  36.8 0.6 reduce-window.18
  37.4 0.2 slice_reduce_fusion
  37.8 0.1 reduce_sum.67
  38.0 9.5 %all-gather.2 = f32[8,1,4]{2,1,0:T(1,128)S(1)} all-gather(f32[1,1,4]{2,1,0:T(1,128)S(1)} %bitcast.270), channel_id=1, replica_groups=mesh['sp'=8,'tp'=4] {'sp'}, dimensions={0}, use_global_device_ids=true | all-gather | bytes 144 | tf_op jit(solution)/shard_map/all_gather | solution.py:18
  47.5 10.1 %all-gather.1 = f32[8,1,4]{2,1,0:T(1,128)S(1)} all-gather(f32[1,1,4]{2,1,0:T(1,128)S(1)} %get-tuple-element.235), channel_id=1, replica_groups=mesh['sp'=8,'tp'=4] {'sp'}, dimensions={0}, use_global_device_ids=true | all-gather | bytes 144 | tf_op jit(solution)/shard_map/all_gather | solution.py:18
  57.7 12.8 %all_gather.53 = f32[8,4,128]{2,1,0:T(4,128)S(1)} all-gather(f32[1,4,128]{2,1,0:T(4,128)S(1)} %bitcast.267), channel_id=1, replica_groups=mesh['sp'=8,'tp'=4] {'sp'}, dimensions={0}, use_global_device_ids=true | all-gather | bytes 18432 | tf_op jit(solution)/shard_map/all_gather | solution.py:18
  70.6 0.2 fusion.63
  71.1 0.2 reduce-window.14
  71.4 0.2 add_maximum_fusion
  71.6 0.4 fusion.82
  72.0 0.3 convolution_bitcast_fusion.1
  72.3 0.2 fusion.83
  72.5 0.4 multiply_reduce_fusion.1
  73.1 9.6 %all_gather.54 = bf16[128,2048]{0,1:T(8,128)(2,1)S(1)} all-gather(bf16[128,512]{0,1:T(8,128)(2,1)S(1)} %bitcast.254), channel_id=1, replica_groups=mesh['sp'=8,'tp'=4] {'tp'}, dimensions={1}, use_global_device_ids=true | all-gather | bytes 655360 | tf_op jit(solution)/shard_map/all_gather | solution.py:193
  82.7 3.0 multiply_reduce_fusion
  85.8 9.0 %psum.7 = f32[128]{0:T(128)S(1)} all-reduce(f32[128]{0:T(128)S(1)} %get-tuple-element.252), channel_id=1, replica_groups=mesh['sp'=8,'tp'=4] {'tp'}, use_global_device_ids=true, to_apply=%region_17.18 | all-reduce | flops 128 | bytes 1024 | tf_op jit(solution)/shard_map/psum | solution.py:211
  94.7 0.5 convolution_convert_fusion
  95.3 67.8 %all_to_all.10 = bf16[8,1,64,1024]{3,2,1,0:T(8,128)(2,1)} all-to-all(bf16[8,1,64,1024]{3,2,1,0:T(8,128)(2,1)S(1)} %bitcast.247), channel_id=1, replica_groups=mesh['sp'=8,'tp'=4] {'sp'}, dimensions={0} | all-to-all | bytes 2097152 | tf_op jit(solution)/shard_map/all_to_all | solution.py:217
  163.1 50.6 %all-gather.7.cloned.1.call-done = bf16[8,1,64,4096]{3,2,0,1:T(8,128)(2,1)} async-done(((bf16[8,1,64,1024]{3,2,0,1:T(8,128)(2,1)}), bf16[8,1,64,4096]{3,2,0,1:T(8,128)(2,1)}) %all-gather.7.cloned.1.call-update) | async-done | bytes 4194320 | tf_op jit(solution)/shard_map/all_gather | solution.py:216
  213.7 5.9 %fusion.26 = f32[8,1,64,512]{3,2,0,1:T(8,128)S(1)} fusion(bf16[1,4096,512]{2,1,0:T(8,128)(2,1)} %param.33, bf16[8,1,64,4096]{3,2,0,1:T(8,128)(2,1)} %all-gather.7.cloned.1.call-done), kind=kOutput, calls=%fused_computation.33 | convolution fusion | flops 2147483648 | bytes 9437184 | tf_op jit(solution)/shard_map/sqid,qdf->sqif/dot_general | solution.py:143
  219.7 3.2 %fusion.41 = bf16[8,1,64,512]{3,2,0,1:T(8,128)(2,1)} fusion(bf16[1,4096,512]{2,1,0:T(8,128)(2,1)S(1)} %copy-done.8, bf16[8,1,64,4096]{3,2,0,1:T(8,128)(2,1)S(1)} %copy-done.9, f32[8,1,64,512]{3,2,0,1:T(8,128)S(1)} %fusion.26), kind=kOutput, calls=%fused_computation.36 | convolution fusion | flops 2149056512 | bytes 9961472 | tf_op jit(solution)/shard_map/sqid,qdf->sqif/dot_general | solution.py:146
  222.9 35.2 %all-gather.9.cloned.1.call-done = bf16[8,1,64,2048]{3,2,0,1:T(8,128)(2,1)} async-done(((bf16[8,1,64,512]{3,2,0,1:T(8,128)(2,1)}), bf16[8,1,64,2048]{3,2,0,1:T(8,128)(2,1)}) %all-gather.9.cloned.1.call-update) | async-done | bytes 2097168 | tf_op jit(solution)/shard_map/all_gather | solution.py:150
  258.1 6.1 %fusion.21 = bf16[8,1,64,1024]{3,2,1,0:T(8,128)(2,1)} fusion(bf16[1,2048,1024]{2,1,0:T(8,128)(2,1)} %param.35, bf16[8,1,64,2048]{3,2,0,1:T(8,128)(2,1)} %all-gather.9.cloned.1.call-done), kind=kOutput, calls=%fused_computation.32 | convolution fusion | flops 2148007936 | bytes 7340032 | tf_op jit(solution)/shard_map/sqif,qfe->sqie/dot_general | solution.py:148
  264.3 4.6 %all-to-all-start.1 = ((bf16[8,1,64,1024]{3,2,1,0:T(8,128)(2,1)}), bf16[8,1,64,1024]{3,2,1,0:T(8,128)(2,1)S(1)}, u32[]{:S(2)}, u32[]{:S(2)}) async-start(bf16[8,1,64,1024]{3,2,1,0:T(8,128)(2,1)} %fusion.21), calls=%async_computation.1 | async-start | bytes 2097152 | tf_op jit(solution)/shard_map/all_to_all | solution.py:223
  268.9 26.5 %all-to-all-done.1 = bf16[8,1,64,1024]{3,2,1,0:T(8,128)(2,1)S(1)} async-done(((bf16[8,1,64,1024]{3,2,1,0:T(8,128)(2,1)}), bf16[8,1,64,1024]{3,2,1,0:T(8,128)(2,1)S(1)}, u32[]{:S(2)}, u32[]{:S(2)}) %all-to-all-start.1) | async-done | bytes 1048608 | tf_op jit(solution)/shard_map/all_to_all | solution.py:223
  295.4 0.4 fusion.47
  295.8 1.1 fusion.48
  (61 shorter events, 1.6 us)
Async XLA Ops:
  6.5 64.0 %copy-start.2 = (s32[128]{0:T(128)S(1)}, s32[128]{0:T(128)}, u32[]{:S(2)}) copy-start(s32[128]{0:T(128)} %param.26) | copy-start | bytes 1540
  6.5 64.1 %copy-start.3 = (f32[128,4]{0,1:T(4,128)S(1)}, f32[128,4]{0,1:T(4,128)}, u32[]{:S(2)}) copy-start(f32[128,4]{0,1:T(4,128)} %param.23) | copy-start | bytes 6148
  6.5 51.1 %copy-start = (bf16[128,512]{1,0:T(8,128)(2,1)S(1)}, bf16[128,512]{1,0:T(8,128)(2,1)}, u32[]{:S(2)}) copy-start(bf16[128,512]{1,0:T(8,128)(2,1)} %param.20) | copy-start | bytes 393220
  6.5 63.9 %copy-start.4 = (s32[128,2]{0,1:T(2,128)S(1)}, s32[128,2]{0,1:T(2,128)}, u32[]{:S(2)}) copy-start(s32[128,2]{0,1:T(2,128)} %param.31) | copy-start | bytes 3076
  6.5 31.4 %copy-start.6 = (bf16[1024]{0:T(1024)(128)(2,1)S(1)}, bf16[1024]{0:T(1024)(128)(2,1)}, u32[]{:S(2)}) copy-start(bf16[1024]{0:T(1024)(128)(2,1)} %param.30) | copy-start | bytes 6148
  6.5 64.3 %all-gather.11.cloned.1.call-start = ((), (), s32[]{:S(2)}) async-start(), calls=%async_computation.4 | async-start | bytes 2359296 | tf_op jit(solution)/shard_map/all_gather | solution.py:18
  20.6 193.2 %all-gather.7.cloned.1.call-start = ((), (), s32[]{:S(2)}) async-start(), calls=%async_computation.2 | async-start | bytes 5242880 | tf_op jit(solution)/shard_map/all_gather | solution.py:216
  57.7 15.3 %copy-start.5 = (f32[512]{0:T(512)S(1)}, f32[512]{0:T(512)}, u32[]{:S(2)}) copy-start(f32[512]{0:T(512)} %param.27) | copy-start | bytes 6148
  70.9 11.8 %copy-start.1 = (bf16[128,1024]{1,0:T(8,128)(2,1)S(1)}, bf16[128,1024]{1,0:T(8,128)(2,1)}, u32[]{:S(2)}) copy-start(bf16[128,1024]{1,0:T(8,128)(2,1)} %param.28) | copy-start | bytes 786436
  163.1 95.1 %all-gather.9.cloned.1.call-start = ((), (), s32[]{:S(2)}) async-start(), calls=%async_computation.3 | async-start | bytes 2621440 | tf_op jit(solution)/shard_map/all_gather | solution.py:150
  213.7 5.9 %copy-start.8 = (bf16[1,4096,512]{2,1,0:T(8,128)(2,1)S(1)}, bf16[1,4096,512]{2,1,0:T(8,128)(2,1)}, u32[]{:S(2)}) copy-start(bf16[1,4096,512]{2,1,0:T(8,128)(2,1)} %param.34) | copy-start | bytes 12582916
  213.7 5.9 %copy-start.9 = (bf16[8,1,64,4096]{3,2,0,1:T(8,128)(2,1)S(1)}, bf16[8,1,64,4096]{3,2,0,1:T(8,128)(2,1)}, u32[]{:S(2)}) copy-start(bf16[8,1,64,4096]{3,2,0,1:T(8,128)(2,1)} %all-gather.7.cloned.1.call-done) | copy-start | bytes 12582916
  222.9 46.0 %copy-start.7 = (f32[128,2]{0,1:T(2,128)S(1)}, f32[128,2]{0,1:T(2,128)}, u32[]{:S(2)}) copy-start(f32[128,2]{0,1:T(2,128)} %param.32) | copy-start | bytes 3076
  264.3 31.2 %all-to-all-start.1 = ((bf16[8,1,64,1024]{3,2,1,0:T(8,128)(2,1)}), bf16[8,1,64,1024]{3,2,1,0:T(8,128)(2,1)S(1)}, u32[]{:S(2)}, u32[]{:S(2)}) async-start(bf16[8,1,64,1024]{3,2,1,0:T(8,128)(2,1)} %fusion.21), calls=%async_computation.1 | async-start | bytes 2097152 | tf_op jit(solution)/shard_map/all_to_all | solution.py:223
Sparse Core Ops, SparseCore 0:
  20.7 31.9 all-gather.10
  163.2 50.5 all-gather.6
  223.1 35.0 all-gather.8
where the time goes:
time: 304 us; the launch traced here: 303 us
  blocking collectives  129 us (42%)
  waiting for transfers between devices  112 us (37%)
  matrix products  22.8 us (8%)
  between operations  14.1 us (5%)
  local copies, waits for them, and re-layouts  10.6 us (3%)
  other arithmetic  9.33 us (3%)
  starting transfers between devices  4.73 us (2%)
    all_to_all x1, blocking collectives, per_device(): lax.all_to_all(packed, 'sp', split_axis=0, concat_axis=0, tiled=True)  67.8 us
    all_gather x1, waiting for transfers between devices, per_device(): lax.all_gather(lax.all_to_all(packed, 'sp', split_axis=0, concat_axis=0,...  50.6 us
    all_gather x1, waiting for transfers between devices, expert_work(): lax.all_gather(hidden, 'tp', axis=3, tiled=True)  35.2 us
    all_gather x3, blocking collectives, prefix_2(): gathered = jax.tree.map(lambda a: lax.all_gather(a, axis), part)  32.4 us
    all_to_all x1, waiting for transfers between devices, per_device(): lax.all_to_all(served, 'sp', split_axis=0, concat_axis=0, tiled=True)  26.5 us
    unnamed x1, blocking collectives  10.6 us
    all_gather x1, blocking collectives, per_device(): lax.all_gather(memory_cell_output, 'tp', axis=1, tiled=True)  9.63 us
    psum x1, blocking collectives, per_device(): squares = lax.psum(jnp.sum(rows_f * rows_f, axis=1), 'tp')  8.98 us
  transfers between devices with their start and end apart: 4, of which 3 were waited for; matrix products, arithmetic and copies ran while one was open for 2% of the time, Pallas kernels for 0%

commit v1 on v0

--- a/solution.py
+++ b/solution.py
@@ -1,6 +1,10 @@
+import functools
+
 import jax
 import jax.numpy as jnp
 from jax import lax
+from jax.experimental import pallas as pl
+from jax.experimental.pallas import tpu as pltpu
 from jax.sharding import PartitionSpec as P
 
 D = 4096
@@ -139,19 +143,256 @@
     return scaled.reshape(length, heads * width).astype(jnp.bfloat16)
 
 
-def expert_work(row_block, gate_weight, up_weight, down_weight):
-    gate_act = jnp.einsum(
-        "sqid,qdf->sqif", row_block, gate_weight, preferred_element_type=jnp.float32
-    )
-    upward = jnp.einsum("sqid,qdf->sqif", row_block, up_weight, preferred_element_type=jnp.float32)
-    hidden = (jax.nn.silu(gate_act) * upward).astype(jnp.bfloat16)
-    result = jnp.einsum(
-        "sqif,qfe->sqie",
-        lax.all_gather(hidden, "tp", axis=3, tiled=True),
-        down_weight,
-        preferred_element_type=jnp.float32,
-    )
-    return result.astype(jnp.bfloat16)
+MESH = pl.DeviceIdType.MESH
+PARALLEL_LIMIT = 56 * 1024 * 1024
+
+
+def remote(src, dst, send, recv, where):
+    return pltpu.make_async_remote_copy(src, dst, send, recv, device_id=where, device_id_type=MESH)
+
+
+def spread_own(teams, j, buf, row, height, width, chunk, send, recv):
+    view = buf.at[pl.ds(row, height), pl.ds(pl.multiple_of(j * width, 128), width)]
+    copies = []
+    if teams == 4:
+        for turn, peer in enumerate((j + 1 - 2 * lax.rem(j, 2), lax.rem(j + 2, 4))):
+            copies.append(remote(view, view, send.at[chunk, turn], recv.at[chunk, turn], {"tp": peer}))
+    else:
+        for turn in range(teams - 1):
+            peer = lax.rem(j + turn + 1, teams)
+            copies.append(remote(view, view, send.at[chunk, turn], recv.at[chunk, turn], {"tp": peer}))
+    return copies
+
+
+def spread_relay(teams, j, buf, row, height, width, chunk, send, recv):
+    if teams != 4:
+        return []
+    half = height // 2
+    across, along = j + 1 - 2 * lax.rem(j, 2), lax.rem(j + 2, 4)
+    first = buf.at[pl.ds(row, half), pl.ds(pl.multiple_of(across * width, 128), width)]
+    second = buf.at[pl.ds(row + half, half), pl.ds(pl.multiple_of(along * width, 128), width)]
+    return [
+        remote(first, first, send.at[chunk, 2], recv.at[chunk, 2], {"tp": along}),
+        remote(second, second, send.at[chunk, 3], recv.at[chunk, 3], {"tp": across}),
+    ]
+
+
+def expert_kernel(
+    groups, teams, cap, each, chunks,
+    normed, resid, chooser, selectors, weights, gate_hbm, up_hbm, down_hbm,
+    out, packed, rows, hidden, result, returned, gate, up, down,
+    load_sem, z_send, z_recv, t_send, t_recv, h_send, h_recv, r_send, r_recv,
+):
+    g, j = lax.axis_index("sp"), lax.axis_index("tp")
+    own_chunk = g // each
+    tall = each * cap
+    width = normed.shape[1]
+    hide = gate.shape[1]
+    loads = [
+        pltpu.make_async_copy(gate_hbm.at[0], gate, load_sem.at[0]),
+        pltpu.make_async_copy(up_hbm.at[0], up, load_sem.at[1]),
+        pltpu.make_async_copy(down_hbm.at[0], down, load_sem.at[2]),
+    ]
+    for load in loads:
+        load.start()
+    barrier = pltpu.get_barrier_semaphore()
+    for step in range(1, groups):
+        pl.semaphore_signal(
+            barrier, inc=1, device_id={"sp": lax.rem(g + step, groups)}, device_id_type=MESH
+        )
+    if teams == 4:
+        peers = (j + 1 - 2 * lax.rem(j, 2), lax.rem(j + 2, 4))
+    else:
+        peers = tuple(lax.rem(j + step, teams) for step in range(1, teams))
+    for peer in peers:
+        pl.semaphore_signal(barrier, inc=1, device_id={"tp": peer}, device_id_type=MESH)
+    packed[...] = jnp.dot(chooser[...], normed[...], preferred_element_type=jnp.float32).astype(
+        jnp.bfloat16
+    )
+    own = pl.ds(pl.multiple_of(g * cap, cap), cap)
+    mine = pl.ds(pl.multiple_of(j * width, 128), width)
+    rows[own, mine] = packed[own, :]
+    pl.semaphore_wait(barrier, groups - 1 + len(peers))
+
+    def dispatch(target):
+        return remote(
+            packed.at[pl.ds(pl.multiple_of(target * cap, cap), cap)],
+            rows.at[own, mine],
+            z_send.at[target],
+            z_recv.at[g],
+            {"sp": target},
+        )
+
+    def give_back(target):
+        return remote(
+            result.at[pl.ds(pl.multiple_of(target * cap, cap), cap)],
+            returned.at[own],
+            r_send.at[target],
+            r_recv.at[g],
+            {"sp": target},
+        )
+
+    def over_others(body):
+        def one(turn, carry):
+            target = lax.rem(own_chunk - turn // each + chunks, chunks) * each + lax.rem(turn, each)
+
+            @pl.when(target != g)
+            def _():
+                body(target)
+
+            return carry
+
+        lax.fori_loop(0, groups, one, 0)
+
+    over_others(lambda target: dispatch(target).start())
+
+    def stage(i, carry):
+        def chunk_of(k):
+            return lax.rem(own_chunk + k, chunks)
+
+        @pl.when(i < chunks)
+        def _():
+            c = chunk_of(i)
+            row = pl.multiple_of(c * tall, tall)
+            for p in range(each):
+                source = c * each + p
+
+                @pl.when(source != g)
+                def _():
+                    place = rows.at[pl.ds(pl.multiple_of(source * cap, cap), cap), mine]
+                    remote(place, place, z_send.at[source], z_recv.at[source], {"sp": source}).wait_recv()
+
+            for copy in spread_own(teams, j, rows, row, tall, width, c, t_send, t_recv):
+                copy.start()
+
+        @pl.when((i >= 1) & (i < chunks + 1))
+        def _():
+            c = chunk_of(i - 1)
+            row = pl.multiple_of(c * tall, tall)
+            for copy in spread_own(teams, j, rows, row, tall, width, c, t_send, t_recv):
+                copy.wait_recv()
+            for copy in spread_relay(teams, j, rows, row, tall, width, c, t_send, t_recv):
+                copy.start()
+
+        @pl.when((i >= 2) & (i < chunks + 2))
+        def _():
+            c = chunk_of(i - 2)
+            row = pl.multiple_of(c * tall, tall)
+            for copy in spread_relay(teams, j, rows, row, tall, width, c, t_send, t_recv):
+                copy.wait_recv()
+
+            @pl.when(i == 2)
+            def _():
+                for load in loads:
+                    load.wait()
+
+            block = rows[pl.ds(row, tall), :]
+            opened = jnp.dot(block, gate[...], preferred_element_type=jnp.float32)
+            raised = jnp.dot(block, up[...], preferred_element_type=jnp.float32)
+            made = (opened * jax.nn.sigmoid(opened) * raised).astype(jnp.bfloat16)
+            hidden[pl.ds(row, tall), pl.ds(pl.multiple_of(j * hide, 128), hide)] = made
+            for copy in spread_own(teams, j, hidden, row, tall, hide, c, h_send, h_recv):
+                copy.start()
+
+        @pl.when((i >= 3) & (i < chunks + 3))
+        def _():
+            c = chunk_of(i - 3)
+            row = pl.multiple_of(c * tall, tall)
+            for copy in spread_own(teams, j, hidden, row, tall, hide, c, h_send, h_recv):
+                copy.wait_recv()
+            for copy in spread_relay(teams, j, hidden, row, tall, hide, c, h_send, h_recv):
+                copy.start()
+
+        @pl.when(i >= 4)
+        def _():
+            c = chunk_of(i - 4)
+            row = pl.multiple_of(c * tall, tall)
+            for copy in spread_relay(teams, j, hidden, row, tall, hide, c, h_send, h_recv):
+                copy.wait_recv()
+            result[pl.ds(row, tall), :] = jnp.dot(
+                hidden[pl.ds(row, tall), :], down[...], preferred_element_type=jnp.float32
+            ).astype(jnp.bfloat16)
+            for p in range(each):
+                target = c * each + p
+
+                @pl.when(target != g)
+                def _():
+                    give_back(target).start()
+
+                @pl.when(target == g)
+                def _():
+                    returned[own, :] = result[own, :]
+
+        return carry
+
+    lax.fori_loop(0, chunks + 4, stage, 0)
+
+    def await_back(source):
+        place = returned.at[pl.ds(pl.multiple_of(source * cap, cap), cap)]
+        remote(place, place, r_send.at[source], r_recv.at[source], {"sp": source}).wait_recv()
+
+    over_others(await_back)
+    mixed = resid[...].astype(jnp.float32)
+    for ordinal in range(TOPK):
+        picked = jnp.dot(selectors[ordinal], returned[...], preferred_element_type=jnp.float32)
+        mixed = mixed + weights[:, ordinal : ordinal + 1] * picked
+    out[...] = mixed.astype(jnp.bfloat16)
+
+    over_others(lambda target: dispatch(target).wait_send())
+    over_others(lambda target: give_back(target).wait_send())
+
+    def drain(c, carry):
+        row = pl.multiple_of(c * tall, tall)
+        for spread in (spread_own, spread_relay):
+            for copy in spread(teams, j, rows, row, tall, width, c, t_send, t_recv):
+                copy.wait_send()
+            for copy in spread(teams, j, hidden, row, tall, hide, c, h_send, h_recv):
+                copy.wait_send()
+        return carry
+
+    lax.fori_loop(0, chunks, drain, 0)
+
+
+def experts(normed, resid, chooser, selectors, weights, gate_weight, up_weight, down_weight, cap):
+    groups, teams = lax.axis_size("sp"), lax.axis_size("tp")
+    slots = groups * cap
+    each = max(1, min(groups, 128 // cap))
+    chunks = groups // each
+    tokens, width = normed.shape
+    _, model, hide = gate_weight.shape
+    _, hidden_all, _ = down_weight.shape
+    ways = max(4, teams)
+    vmem = pl.BlockSpec(memory_space=pltpu.VMEM)
+    hbm = pl.BlockSpec(memory_space=pl.ANY)
+    bf16 = jnp.bfloat16
+    return pl.pallas_call(
+        functools.partial(expert_kernel, groups, teams, cap, each, chunks),
+        out_shape=jax.ShapeDtypeStruct((tokens, width), bf16),
+        in_specs=[vmem] * 5 + [hbm] * 3,
+        out_specs=vmem,
+        scratch_shapes=[
+            pltpu.VMEM((slots, width), bf16),
+            pltpu.VMEM((slots, model), bf16),
+            pltpu.VMEM((slots, hidden_all), bf16),
+            pltpu.VMEM((slots, width), bf16),
+            pltpu.VMEM((slots, width), bf16),
+            pltpu.VMEM((model, hide), bf16),
+            pltpu.VMEM((model, hide), bf16),
+            pltpu.VMEM((hidden_all, width), bf16),
+            pltpu.SemaphoreType.DMA((3,)),
+            pltpu.SemaphoreType.DMA((groups,)),
+            pltpu.SemaphoreType.DMA((groups,)),
+            pltpu.SemaphoreType.DMA((chunks, ways)),
+            pltpu.SemaphoreType.DMA((chunks, ways)),
+            pltpu.SemaphoreType.DMA((chunks, ways)),
+            pltpu.SemaphoreType.DMA((chunks, ways)),
+            pltpu.SemaphoreType.DMA((groups,)),
+            pltpu.SemaphoreType.DMA((groups,)),
+        ],
+        compiler_params=pltpu.CompilerParams(
+            collective_id=1, has_side_effects=True, vmem_limit_bytes=PARALLEL_LIMIT
+        ),
+    )(normed, resid, chooser, selectors, weights, gate_weight, up_weight, down_weight)
 
 
 def per_device(
@@ -206,29 +447,14 @@
     slot_of = (flat_ids * capacity + rank_in).reshape(tokens, TOPK)
     slot_index = jnp.arange(experts_all * capacity, dtype=jnp.int32)
     chooser = jnp.any(slot_index[:, None, None] == slot_of[None, :, :], axis=2).astype(jnp.bfloat16)
-    bucket_shape = (groups, gate_weight.shape[0], capacity)
     rows_f = resid.astype(jnp.float32)
     squares = lax.psum(jnp.sum(rows_f * rows_f, axis=1), "tp")
     normed = rows_f * lax.rsqrt(squares[:, None] / D + EPSILON)
     normed = (normed * expert_norm_gain.astype(jnp.float32)[None, :]).astype(jnp.bfloat16)
-    packed = jnp.dot(chooser, normed, preferred_element_type=jnp.float32).astype(jnp.bfloat16)
-    packed = packed.reshape(bucket_shape + (normed.shape[1],))
-    row_block = lax.all_gather(
-        lax.all_to_all(packed, "sp", split_axis=0, concat_axis=0, tiled=True),
-        "tp",
-        axis=3,
-        tiled=True,
-    )
-    served = expert_work(row_block, gate_weight, up_weight, down_weight)
-    returned = lax.all_to_all(served, "sp", split_axis=0, concat_axis=0, tiled=True).reshape(
-        -1, served.shape[3]
-    )
-    mixed = resid.astype(jnp.float32)
-    for ordinal in range(TOPK):
-        selector = (slot_of[:, ordinal][:, None] == slot_index[None, :]).astype(jnp.bfloat16)
-        picked = jnp.dot(selector, returned, preferred_element_type=jnp.float32)
-        mixed = mixed + routing_weight[:, ordinal : ordinal + 1] * picked
-    return mixed.astype(jnp.bfloat16)
+    selectors = (slot_of.T[:, :, None] == slot_index[None, None, :]).astype(jnp.bfloat16)
+    return experts(
+        normed, resid, chooser, selectors, routing_weight, gate_weight, up_weight, down_weight, capacity
+    )
 
 
 def solution(mesh):

time: 304 us -> 224 us (0.74)
  Pallas kernels: 0 us -> 114 us
  waiting for transfers between devices: 112 us -> 0.02 us
  blocking collectives: 129 us -> 61.6 us
  matrix products: 22.8 us -> 5.6 us
  starting transfers between devices: 4.73 us -> 0.04 us
    pallas_call x0 -> x1, Pallas kernels: none -> 114 us  [experts(): pl.pallas_call(functools.partial(expert_kernel, groups, teams, cap, each,...]
    all_gather x2 -> x0, waiting for transfers between devices: 85.8 us -> none  [the longest x1 50.6 us: per_device(): lax.all_gather(lax.all_to_all(packed, 'sp', split_axis=0, concat_axis=0,...]
    all_to_all x1 -> x0, blocking collectives: 67.8 us -> none  [per_device(): lax.all_to_all(packed, 'sp', split_axis=0, concat_axis=0, tiled=True)]
    all_to_all x1 -> x0, waiting for transfers between devices: 26.5 us -> none  [per_device(): lax.all_to_all(served, 'sp', split_axis=0, concat_axis=0, tiled=True)]
    dot_general x6 -> x0, matrix products: 17.2 us -> none  [the longest x1 6.14 us: expert_work(): jnp.einsum('sqif,qfe->sqie', lax.all_gather(hidden, 'tp', axis=3, tiled=T...]
    all_to_all x1 -> x0, starting transfers between devices: 4.61 us -> none  [per_device(): lax.all_to_all(served, 'sp', split_axis=0, concat_axis=0, tiled=True)]
    unnamed x28 -> x26, local copies, waits for them, and re-layouts: 6.26 us -> 8.67 us
  transfers between devices with their start and end apart: 4 -> 1, of which waited for: 3 -> 0; matrix products, arithmetic and copies ran while one was open for 2% -> 5% of each run, Pallas kernels for 0% -> 0%
where the time goes in v1:
time: 224 us; the launch traced here: 221 us
  Pallas kernels  114 us (51%)
  blocking collectives  61.6 us (28%)
  between operations  14.3 us (6%)
  local copies, waits for them, and re-layouts  13 us (6%)
  other arithmetic  12.3 us (5%)
  matrix products  5.6 us (2%)
    pallas_call x1, Pallas kernels, experts(): pl.pallas_call(functools.partial(expert_kernel, groups, teams, cap, each,...  114 us
    all_gather x3, blocking collectives, prefix_2(): gathered = jax.tree.map(lambda a: lax.all_gather(a, axis), part)  31.9 us
    unnamed x1, blocking collectives  10.6 us
    all_gather x1, blocking collectives, per_device(): lax.all_gather(memory_cell_output, 'tp', axis=1, tiled=True)  10.1 us
    psum x1, blocking collectives, per_device(): squares = lax.psum(jnp.sum(rows_f * rows_f, axis=1), 'tp')  8.98 us
    unnamed x26, local copies, waits for them, and re-layouts  8.67 us
  transfers between devices with their start and end apart: 1, of which 0 were waited for; matrix products, arithmetic and copies ran while one was open for 5% of the time, Pallas kernels for 0%

profile of v1, /device:TPU:0, one launch (start us, length us, event | category | flops | bytes accessed | tf_op | source)
XLA Modules:
  0.0 220.6 jit_solution(13574650342252286373)
XLA Ops:
  6.6 0.7 fusion.31
  7.5 0.2 reduce_window_sum.27
  7.7 1.5 fusion.38
  9.2 1.2 dynamic-slice
  10.4 2.0 slice_dynamic-update-slice_fusion
  12.5 1.3 broadcast_compare_fusion.1
  13.8 0.7 fusion.35
  14.5 0.6 iota_compare_fusion.7
  15.7 0.9 select_reduce_fusion
  16.6 0.8 select_multiply_fusion
  17.4 1.0 copy.152
  18.4 1.0 copy.158
  19.4 1.1 fusion.20
  20.6 0.7 dynamic-update-slice.1
  21.3 1.4 slice_dynamic-update-slice_fusion.1
  22.7 10.6 %all-reduce.3 = (s32[8]{0:T(128)S(1)}, s32[8]{0:T(128)S(1)}, s32[8]{0:T(128)S(1)}) all-reduce(s32[8]{0:T(128)S(1)} %slice_dynamic-update-slice_fusion.1, s32[8]{0:T(128)S(1)} %dynamic-update-slice.1, s32[8]{0:T(128)S(1)} %get-tuple-element.227), channel_id=1, replica_groups=mesh['sp'=8,'tp'=4] {'sp'}, use_global_device_ids=true, to_apply=%add | all-reduce | flops 24 | bytes 192
  33.4 0.8 copy.139
  34.2 0.1 eq.113
  34.3 0.1 eq.109
  34.5 0.1 copy.150
  34.6 1.0 copy.151
  35.6 1.0 add_divide_fusion
  36.6 0.1 copy.119
  36.8 0.7 convert_element_type.52
  37.5 0.6 reduce-window.18
  38.0 0.2 slice_reduce_fusion
  38.4 0.1 reduce_sum.68
  38.7 0.7 convert_element_type.56.chooser
  39.4 0.7 copy.142.weights
  40.1 9.5 %all-gather.2 = f32[8,1,4]{2,1,0:T(1,128)S(1)} all-gather(f32[1,1,4]{2,1,0:T(1,128)S(1)} %bitcast.184), channel_id=1, replica_groups=mesh['sp'=8,'tp'=4] {'sp'}, dimensions={0}, use_global_device_ids=true | all-gather | bytes 144 | tf_op jit(solution)/shard_map/all_gather | solution.py:22
  49.6 9.6 %all-gather.1 = f32[8,1,4]{2,1,0:T(1,128)S(1)} all-gather(f32[1,1,4]{2,1,0:T(1,128)S(1)} %get-tuple-element.222), channel_id=1, replica_groups=mesh['sp'=8,'tp'=4] {'sp'}, dimensions={0}, use_global_device_ids=true | all-gather | bytes 144 | tf_op jit(solution)/shard_map/all_gather | solution.py:22
  59.3 12.8 %all_gather.47 = f32[8,4,128]{2,1,0:T(4,128)S(1)} all-gather(f32[1,4,128]{2,1,0:T(4,128)S(1)} %bitcast.181), channel_id=1, replica_groups=mesh['sp'=8,'tp'=4] {'sp'}, dimensions={0}, use_global_device_ids=true | all-gather | bytes 18432 | tf_op jit(solution)/shard_map/all_gather | solution.py:22
  72.1 0.2 fusion.22
  72.4 0.8 fusion.18.selectors
  73.4 0.1 copy.133
  73.5 0.2 reduce-window.14
  73.8 0.2 add_maximum_fusion
  74.0 0.4 fusion.39
  74.3 0.3 convolution_bitcast_fusion.1
  74.6 0.2 fusion.40
  74.8 0.4 multiply_reduce_fusion
  75.3 0.1 multiply_convert_fusion
  75.4 10.1 %all_gather.48 = bf16[128,2048]{0,1:T(8,128)(2,1)S(1)} all-gather(bf16[128,512]{0,1:T(8,128)(2,1)S(1)} %bitcast.167), channel_id=1, replica_groups=mesh['sp'=8,'tp'=4] {'tp'}, dimensions={1}, use_global_device_ids=true | all-gather | bytes 655360 | tf_op jit(solution)/shard_map/all_gather | solution.py:434
  85.5 3.0 %fusion.14 = (f32[128]{0:T(128)S(1)}, bf16[128,1024]{1,0:T(8,128)(2,1)S(1)}) fusion(bf16[128,2048]{0,1:T(8,128)(2,1)S(1)} %all_gather.48, bf16[2048,1024]{1,0:T(8,128)(2,1)} %param.29, bf16[128,1024]{1,0:T(8,128)(2,1)S(1)} %copy-done.2), kind=kOutput, calls=%fused_computation.35 | convolution fusion | flops 537657216 | bytes 5243392 | tf_op jit(solution)/shard_map/dot_general | solution.py:433
  88.6 9.0 %psum.7 = f32[128]{0:T(128)S(1)} all-reduce(f32[128]{0:T(128)S(1)} %get-tuple-element.235), channel_id=1, replica_groups=mesh['sp'=8,'tp'=4] {'tp'}, use_global_device_ids=true, to_apply=%region_13.14 | all-reduce | flops 128 | bytes 1024 | tf_op jit(solution)/shard_map/psum | solution.py:451
  97.6 0.8 fusion.16.normed
  98.4 113.7 %shard_map.163 = bf16[128,1024]{1,0:T(8,128)(2,1)} custom-call(bf16[128,1024]{1,0:T(8,128)(2,1)} %fusion.16.normed, bf16[128,1024]{1,0:T(8,128)(2,1)} %copy-done, bf16[512,128]{1,0:T(8,128)(2,1)} %convert_element_type.56.chooser, bf16[2,128,512]{2,1,0:T(8,128)(2,1)} %fusion.18.selectors, f32[128,2]{1,0:T(8,128)} %copy.142.weights, ...), custom_call_target="tpu_custom_call" | custom-call | tf_op jit(solution)/shard_map/pallas_call | solution.py:368
  212.1 1.7 copy.188
  (46 shorter events, 1.0 us)
Async XLA Ops:
  6.5 65.5 %copy-start.3 = (s32[128]{0:T(128)S(1)}, s32[128]{0:T(128)}, u32[]{:S(2)}) copy-start(s32[128]{0:T(128)} %param.26) | copy-start | bytes 1540
  6.5 65.6 %copy-start.4 = (f32[128,4]{0,1:T(4,128)S(1)}, f32[128,4]{0,1:T(4,128)}, u32[]{:S(2)}) copy-start(f32[128,4]{0,1:T(4,128)} %param.23) | copy-start | bytes 6148
  6.5 52.7 %copy-start.1 = (bf16[128,512]{1,0:T(8,128)(2,1)S(1)}, bf16[128,512]{1,0:T(8,128)(2,1)}, u32[]{:S(2)}) copy-start(bf16[128,512]{1,0:T(8,128)(2,1)} %param.20) | copy-start | bytes 393220
  6.5 32.1 %copy-start.5 = (s32[128,2]{0,1:T(2,128)S(1)}, s32[128,2]{0,1:T(2,128)}, u32[]{:S(2)}) copy-start(s32[128,2]{0,1:T(2,128)} %param.31) | copy-start | bytes 3076
  6.5 32.8 %copy-start.7 = (f32[128,2]{0,1:T(2,128)S(1)}, f32[128,2]{0,1:T(2,128)}, u32[]{:S(2)}) copy-start(f32[128,2]{0,1:T(2,128)} %param.32) | copy-start | bytes 3076
  6.5 66.7 %all-gather.5.cloned.1.call-start = ((), (), s32[]{:S(2)}) async-start(), calls=%async_computation | async-start | bytes 2359296 | tf_op jit(solution)/shard_map/all_gather | solution.py:22
  72.4 2.9 %copy-start.6 = (f32[512]{0:T(512)S(1)}, f32[512]{0:T(512)}, u32[]{:S(2)}) copy-start(f32[512]{0:T(512)} %param.27) | copy-start | bytes 6148
  73.2 12.3 %copy-start.2 = (bf16[128,1024]{1,0:T(8,128)(2,1)S(1)}, bf16[128,1024]{1,0:T(8,128)(2,1)}, u32[]{:S(2)}) copy-start(bf16[128,1024]{1,0:T(8,128)(2,1)} %param.28) | copy-start | bytes 786436
  88.6 9.8 %copy-start = (bf16[128,1024]{1,0:T(8,128)(2,1)}, bf16[128,1024]{1,0:T(8,128)(2,1)S(1)}, u32[]{:S(2)}) copy-start(bf16[128,1024]{1,0:T(8,128)(2,1)S(1)} %get-tuple-element.236.resid) | copy-start | bytes 786436
Sparse Core Ops, SparseCore 0:
  20.7 31.8 all-gather.4
